TPU v7x, 32 devices: a whole 2x2x4 slice. The times are simulated.
32 devices in a mesh: sp: 16 (over z, y, x), tp: 2 (over core).
Axes of the slice: x: 2, y: 2, z: 4, core: 2. Of those that a mesh axis runs over, the one named last changes fastest.
Arguments:
- tokens: bfloat16 [1024, 1, 2048], P('sp'), may hold values from -6 to 6
- queries: bfloat16 [1024, 1, 1024], P('sp', None, 'tp'), may hold values from -15 to 15
- key_values: bfloat16 [1024, 1, 1024], P('sp', None, 'tp'), may hold values from -6 to 6
- stop_bias: bfloat16 [1024, 1, 16], P('sp', None, 'tp'), may hold values from -20 to 0
- out_proj: bfloat16 [1024, 2048], P('tp'), may hold values from -0.375 to 0.375
- norm_gain: float32 [2048], replicated, may hold values from 0.1 to 1.9
- up_proj: bfloat16 [2048, 4096], P('sp', 'tp'), may hold values from -0.125 to 0.125
- down_proj: bfloat16 [4096, 2048], P('tp', 'sp'), may hold values from -0.09375 to 0.09375
Outputs:
- layer_out: bfloat16 [1024, 1, 2048], P(('sp', 'tp'))
All inputs are finite; a program needn't handle non-finite values.
Results may differ from a plain program's by a relative error of at most 0.018.
Values may be sent and summed in bfloat16 or wider, within the bound.
A program may use at most 64 MiB of HBM per device.

v0:
```python
import math

import jax
import jax.numpy as jnp
from jax import lax
from jax.experimental import pallas as pl
from jax.experimental.pallas import tpu as pltpu
from jax.sharding import PartitionSpec as P

HEAD = 64


EPSILON = 1e-06


def rms_scale(residual, gain):
    values = residual.astype(jnp.float32)
    factor = lax.rsqrt(jnp.mean(values * values, axis=-1, keepdims=True) + EPSILON)
    return (values * factor * gain).astype(jnp.bfloat16)


def sweep_keys(totals, pieces, shard_rows, step_fn):
    kv_rows, bias_rows = pieces
    shards = kv_rows.shape[0] // shard_rows
    group_shards = math.gcd(shards, max(1, 1024 // shard_rows))
    span_rows = group_shards * shard_rows

    def advance(number, running):
        first_row = number * span_rows
        kv_block = lax.dynamic_slice_in_dim(kv_rows, first_row, span_rows, 0)
        bias_block = lax.dynamic_slice_in_dim(bias_rows, first_row, span_rows, 0)
        return step_fn(running, kv_block, bias_block, first_row, group_shards)

    return lax.fori_loop(0, shards // group_shards, advance, totals)


def general_body(tokens, queries, key_values, stop_bias, out_proj, norm_gain, up_proj, down_proj):
    row_count = tokens.shape[0]
    seq_count = tokens.shape[1]
    head_count = queries.shape[2] // HEAD
    kv_count = key_values.shape[2] // (2 * HEAD)
    group_size = head_count // kv_count
    n_shards = lax.axis_size("sp")
    query_start = lax.axis_index("sp") * row_count
    query_pos = query_start + lax.iota(jnp.int32, row_count)
    q_heads = queries.reshape(row_count, seq_count, kv_count, group_size, HEAD).transpose(
        1, 2, 3, 0, 4
    )
    q_heads = q_heads.reshape(seq_count, kv_count, group_size * row_count, HEAD)

    def stick_block(kv_block, bias_block, key_start):
        span_rows = kv_block.shape[0]
        key_pairs = kv_block.reshape(span_rows, seq_count, kv_count, 2 * HEAD)
        keys_part = key_pairs[..., :HEAD]
        values_part = key_pairs[..., HEAD:]
        scores = (
            jnp.einsum("bgmd,sbgd->bgms", q_heads, keys_part, preferred_element_type=jnp.float32)
            * 0.125
        )
        bias_float = jnp.transpose(bias_block, (1, 2, 0)).astype(jnp.float32)
        scores = (
            scores.reshape(seq_count, head_count, row_count, span_rows) + bias_float[:, :, None, :]
        )
        key_pos = key_start + lax.iota(jnp.int32, span_rows)
        strict = key_pos[None, :] < query_pos[:, None]
        log_pass = jnp.where(strict, jax.nn.log_sigmoid(-scores), 0.0)
        return (scores, strict, log_pass, values_part)

    def weigh(scores, strict, after_sum, values_part):
        span_rows = scores.shape[3]
        weights = jnp.where(strict, jnp.exp(jax.nn.log_sigmoid(scores) + after_sum), 0.0).astype(
            jnp.bfloat16
        )
        weights = weights.reshape(seq_count, kv_count, group_size * row_count, span_rows)
        return jnp.einsum(
            "bgms,sbgd->bgmd", weights, values_part, preferred_element_type=jnp.float32
        )

    empty_out = jnp.zeros((seq_count, kv_count, group_size * row_count, HEAD), jnp.float32)

    def sum_step(sums_table, kv_block, bias_block, key_start, shard_group):

        def sum_compute(table_in):
            scores, strict, log_pass, values_part = stick_block(kv_block, bias_block, key_start)
            block_sums = log_pass.reshape(
                seq_count, head_count, row_count, shard_group, row_count
            ).sum(axis=4)
            slot_index = key_start // row_count
            current = lax.dynamic_slice_in_dim(table_in, slot_index, shard_group, 0)
            return lax.dynamic_update_slice_in_dim(
                table_in, current + jnp.transpose(block_sums, (3, 0, 1, 2)), slot_index, 0
            )

        return lax.cond(
            key_start < query_start + row_count, sum_compute, lambda table_in: table_in, sums_table
        )

    empty_table = jnp.zeros((n_shards, seq_count, head_count, row_count), jnp.float32)
    sums_table = sweep_keys(
        empty_table,
        (
            lax.all_gather(key_values, "sp", axis=0, tiled=True),
            lax.all_gather(stop_bias, "sp", axis=0, tiled=True),
        ),
        row_count,
        sum_step,
    )
    offsets = lax.cumsum(sums_table, axis=0, reverse=True) - sums_table

    def out_step(outputs, kv_block, bias_block, key_start, shard_group):

        def out_compute(running):
            scores, strict, log_pass, values_part = stick_block(kv_block, bias_block, key_start)
            span_rows = kv_block.shape[0]
            split_pass = log_pass.reshape(seq_count, head_count, row_count, shard_group, row_count)
            within = lax.cumsum(split_pass, axis=4, reverse=True) - split_pass
            carried = lax.dynamic_slice_in_dim(offsets, key_start // row_count, shard_group, 0)
            carried = jnp.transpose(carried, (1, 2, 3, 0))[..., None]
            after_sum = (within + carried).reshape(seq_count, head_count, row_count, span_rows)
            return running + weigh(scores, strict, after_sum, values_part)

        return lax.cond(
            key_start < query_start + row_count, out_compute, lambda running: running, outputs
        )

    accum_out = sweep_keys(
        empty_out,
        (
            lax.all_gather(key_values, "sp", axis=0, tiled=True),
            lax.all_gather(stop_bias, "sp", axis=0, tiled=True),
        ),
        row_count,
        out_step,
    )
    attended = accum_out.reshape(seq_count, kv_count, group_size, row_count, HEAD).transpose(
        3, 0, 1, 2, 4
    )
    attended = attended.reshape(row_count * seq_count, head_count * HEAD).astype(jnp.bfloat16)
    share_tokens = row_count // lax.axis_size("tp")
    share_rows = share_tokens * seq_count
    tp_index = lax.axis_index("tp")
    projected = lax.psum(
        jnp.dot(attended, out_proj, preferred_element_type=jnp.float32).astype(jnp.bfloat16), "tp"
    ).astype(jnp.float32)
    flat_tokens = tokens.reshape(row_count * seq_count, tokens.shape[2])
    residual = (flat_tokens.astype(jnp.float32) + projected).astype(jnp.bfloat16)
    normed = rms_scale(residual, norm_gain)
    residual_share = lax.dynamic_slice_in_dim(residual, tp_index * share_rows, share_rows, 0)
    up_values = jnp.dot(
        normed,
        lax.all_gather(up_proj, "sp", axis=0, tiled=True),
        preferred_element_type=jnp.float32,
    )
    hidden = jnp.square(jax.nn.relu(up_values)).astype(jnp.bfloat16)
    partial_terms = jnp.dot(
        hidden,
        lax.all_gather(down_proj, "sp", axis=1, tiled=True),
        preferred_element_type=jnp.float32,
    )
    update = lax.psum_scatter(
        partial_terms.astype(jnp.bfloat16), "tp", scatter_dimension=0, tiled=True
    ).astype(jnp.float32)
    result = (residual_share.astype(jnp.float32) + update).astype(jnp.bfloat16)
    return result.reshape(share_tokens, seq_count, result.shape[1])


MESH = pl.DeviceIdType.MESH
LO = 4
LANES = 128
F32 = jnp.float32
BF16 = jnp.bfloat16


def remote(src, dst, send, recv, sp, tp):
    return pltpu.make_async_remote_copy(
        src_ref=src,
        dst_ref=dst,
        send_sem=send,
        recv_sem=recv,
        device_id={"sp": sp, "tp": tp},
        device_id_type=MESH,
    )


def dot_nt(a, b):
    return lax.dot_general(a, b, (((1,), (1,)), ((), ())), preferred_element_type=F32)


def dot_tn(a, b):
    return lax.dot_general(a, b, (((0,), (0,)), ((), ())), preferred_element_type=F32)


def layer_kernel(
    HI,
    G,
    tok_ref,
    q_ref,
    kvb_ref,
    wo_ref,
    gain_ref,
    up_ref,
    dn_ref,
    out_ref,
    kv_buf,
    up_buf,
    dn_buf,
    q_buf,
    tri_buf,
    carry,
    acc,
    att_buf,
    pj_buf,
    pj_in,
    res_buf,
    n_buf,
    hid_buf,
    ps_buf,
    pr_buf,
    kv_sz,
    kv_sp,
    kv_recv,
    wz_send,
    wp_send,
    up_recv,
    dn_recv,
    pj_send,
    pj_recv,
    n_send,
    nf_send,
    n_recv,
    p_send,
    p_recv,
):
    s = lax.axis_index("sp")
    c = lax.axis_index("tp")
    hi = s // LO
    lo = s % LO
    lo1 = lo + 1 - 2 * (lo % 2)
    lo2 = (lo + 2) % LO
    lo3 = (lo1 + 2) % LO
    other = 1 - c
    T = q_ref.shape[0]
    H = T // 2
    D = tok_ref.shape[1]
    R = up_ref.shape[0]
    CH = up_buf.shape[1]
    KW = G * LANES
    PL = LO * T

    barrier = pltpu.get_barrier_semaphore()
    for p in (lo1, lo2, lo3):
        pl.semaphore_signal(barrier, inc=1, device_id={"sp": hi * LO + p, "tp": c}, device_id_type=MESH)
    pl.semaphore_signal(barrier, inc=1, device_id={"sp": s, "tp": other}, device_id_type=MESH)
    for dz in range(1, HI):
        far = ((hi + dz) % HI) * LO + lo
        for core in range(2):
            pl.semaphore_signal(barrier, inc=1, device_id={"sp": far, "tp": core}, device_id_type=MESH)
    pl.semaphore_wait(barrier, 4 + 2 * (HI - 1))

    def kv_up(hp):
        return remote(
            kvb_ref, kv_buf.at[pl.ds(s * T, T)], kv_sz.at[hp], kv_recv.at[s], hp * LO + lo, c
        )

    def kv_flat(hp, k, src):
        j = hp * LO + lo
        peer = (lo1, lo2, lo3)[k]
        return remote(
            src, kv_buf.at[pl.ds(j * T, T)], kv_sp.at[hp * 3 + k], kv_recv.at[j], hi * LO + peer, c
        )

    def kv_wait(j):
        block = kv_buf.at[pl.ds(j * T, T)]
        remote(block, block, kv_sz.at[0], kv_recv.at[j], s, other).wait_recv()

    def w_far(dz):
        hp = (hi + dz) % HI
        far = hp * LO + lo
        return (
            remote(
                up_ref.at[:, pl.ds(pl.multiple_of(hp * CH, LANES), CH)],
                up_buf.at[pl.ds(s * R, R)],
                wz_send.at[2 * dz],
                up_recv.at[s],
                far,
                c,
            ),
            remote(
                dn_ref.at[pl.ds(hp * CH, CH)],
                dn_buf.at[s],
                wz_send.at[2 * dz + 1],
                dn_recv.at[s],
                far,
                c,
            ),
        )

    def up_at(j):
        return up_buf.at[pl.ds(j * R, R)]

    def up_wait(j):
        remote(up_at(j), up_at(j), wz_send.at[0], up_recv.at[j], s, other).wait_recv()

    def dn_wait(j):
        remote(dn_buf.at[j], dn_buf.at[j], wz_send.at[0], dn_recv.at[j], s, other).wait_recv()

    def w_flat(dz):
        j = ((hi - dz + HI) % HI) * LO + lo
        if dz == 0:
            up_src = up_ref.at[:, pl.ds(pl.multiple_of(hi * CH, LANES), CH)]
            dn_src = dn_ref.at[pl.ds(hi * CH, CH)]
        else:
            up_src = up_at(j)
            dn_src = dn_buf.at[j]
        copies = []
        for k, peer in enumerate((lo1, lo2)):
            far = hi * LO + peer
            copies.append(remote(up_src, up_at(j), wp_send.at[6 * dz + 2 * k], up_recv.at[j], far, c))
            copies.append(
                remote(dn_src, dn_buf.at[j], wp_send.at[6 * dz + 2 * k + 1], dn_recv.at[j], far, c)
            )
        return copies

    def w_diag(dz):
        row = ((hi - dz + HI) % HI) * LO
        return (
            remote(
                up_at(row + lo1),
                up_at(row + lo1),
                wp_send.at[6 * dz + 4],
                up_recv.at[row + lo1],
                hi * LO + lo2,
                c,
            ),
            remote(
                dn_buf.at[row + lo2],
                dn_buf.at[row + lo2],
                wp_send.at[6 * dz + 5],
                dn_recv.at[row + lo2],
                hi * LO + lo1,
                c,
            ),
        )

    for hp in range(HI):

        @pl.when(hp > hi)
        def _():
            kv_up(hp).start()

    for hp in range(HI):

        @pl.when(hp == hi)
        def _():
            for k in range(3):
                kv_flat(hp, k, kvb_ref).start()

    for dz in range(1, HI):
        for copy in w_far(dz):
            copy.start()

    kv_buf[pl.ds(s * T, T), :] = kvb_ref[...]
    up_buf[pl.ds(s * R, R), :] = up_ref[:, pl.ds(pl.multiple_of(hi * CH, LANES), CH)]
    dn_buf[s] = dn_ref[pl.ds(hi * CH, CH), :]
    row_id = lax.broadcasted_iota(jnp.int32, (PL, PL), 0)
    col_id = lax.broadcasted_iota(jnp.int32, (PL, PL), 1)
    tri_buf[...] = jnp.where(col_id > row_id, 1.0, 0.0).astype(BF16)
    lane = lax.broadcasted_iota(jnp.int32, (T, LANES), 1)
    low = lane < HEAD
    for g in range(G):
        qg = q_ref[:, g * LANES : (g + 1) * LANES].astype(F32) * 0.125
        first = jnp.where(low, qg, 0.0)
        second = jnp.where(low, pltpu.roll(qg, HEAD, 1), 0.0)
        q_buf[g] = jnp.concatenate([first, second], axis=0).astype(BF16)
    carry[...] = jnp.zeros_like(carry)
    acc[...] = jnp.zeros_like(acc)

    for hp in range(HI - 1):

        @pl.when(hp < hi)
        def _():
            kv_wait(hp * LO + lo)
            for k in range(3):
                kv_flat(hp, k, kv_buf.at[pl.ds((hp * LO + lo) * T, T)]).start()

    for copy in w_flat(0):
        copy.start()

    sel_row = lax.broadcasted_iota(jnp.int32, (LANES, LANES), 0) // HEAD
    sel_lane = lax.broadcasted_iota(jnp.int32, (LANES, LANES), 1)
    key_row = lax.broadcasted_iota(jnp.int32, (PL, LANES), 0)
    query_pos = s * T + lax.broadcasted_iota(jnp.int32, (PL, LANES), 1) % T

    def attend(plane):
        for p in (lo1, lo2, lo3):
            kv_wait(plane * LO + p)
        rows = pl.ds(plane * PL, PL)
        bias = kv_buf[rows, KW : KW + LANES]
        strict = plane * PL + key_row < query_pos
        for g in range(G):
            kv = kv_buf[rows, g * LANES : (g + 1) * LANES]
            pick = jnp.where(sel_lane == 2 * g + sel_row, 1.0, 0.0).astype(BF16)
            scores = dot_nt(kv, q_buf[g]) + dot_nt(bias, pick)
            soft = jnp.maximum(scores, 0.0) + jnp.log(1.0 + jnp.exp(-jnp.abs(scores)))
            log_pass = jnp.where(strict, -soft, 0.0)
            top = log_pass.astype(BF16)
            rest = (log_pass - top.astype(F32)).astype(BF16)
            after = jnp.dot(tri_buf[...], top, preferred_element_type=F32) + jnp.dot(
                tri_buf[...], rest, preferred_element_type=F32
            )
            held = carry[g]
            weights = jnp.where(strict, jnp.exp(scores - soft + after + held), 0.0).astype(BF16)
            acc[g] += dot_tn(weights, kv)
            carry[g] = held + after[0:1] + log_pass[0:1]

    for k in range(HI):

        @pl.when(k <= hi)
        def _():
            attend(hi - k)

        if k + 1 < HI:
            j = ((hi - k - 1 + HI) % HI) * LO + lo
            up_wait(j)
            dn_wait(j)
            for copy in w_flat(k + 1):
                copy.start()

    for g in range(G):
        a0 = pltpu.roll(acc[g, 0:T, :], HEAD, 1)
        a1 = acc[g, T : 2 * T, :]
        att_buf[:, g * LANES : (g + 1) * LANES] = jnp.where(low, a0, a1).astype(BF16)
    att = att_buf[...]
    wide = 512 if D % 512 == 0 else LANES

    @pl.loop(0, D // wide)
    def _(i):
        cols = pl.ds(pl.multiple_of(i * wide, wide), wide)
        part = jnp.dot(att, wo_ref[:, cols], preferred_element_type=F32)
        pj_buf[:, cols] = part.astype(BF16)

    pj_copy = remote(pj_buf.at[pl.ds(other * H, H)], pj_in, pj_send, pj_recv, s, other)
    pj_copy.start()
    pj_copy.wait()
    mine = pl.ds(c * H, H)
    total = pj_buf[mine, :].astype(F32) + pj_in[...].astype(F32)
    residual = (tok_ref[mine, :].astype(F32) + total).astype(BF16)
    res_buf[...] = residual
    values = residual.astype(F32)
    factor = lax.rsqrt(jnp.mean(values * values, axis=-1, keepdims=True) + EPSILON)
    me = hi * 2 + c

    def n_at(i):
        return n_buf.at[pl.ds(i * H, H)]

    n_buf[pl.ds(me * H, H), :] = (values * factor * gain_ref[...]).astype(BF16)

    def n_out(dz):
        hp = (hi + dz) % HI
        return remote(n_at(me), n_at(me), n_send.at[dz], n_recv.at[me], hp * LO + lo, c)

    def n_pass(dz):
        i = ((hi - dz + HI) % HI) * 2 + c
        return remote(n_at(i), n_at(i), nf_send.at[dz], n_recv.at[i], s, other)

    def n_wait(i):
        remote(n_at(i), n_at(i), nf_send.at[0], n_recv.at[i], s, other).wait_recv()

    for dz in range(1, HI):
        n_out(dz).start()
    n_pass(0).start()

    for dz in range(HI):
        row = ((hi - dz + HI) % HI) * LO
        up_wait(row + lo1)
        dn_wait(row + lo2)
        for copy in w_diag(dz):
            copy.start()
    for dz in range(1, HI):
        n_wait(((hi - dz + HI) % HI) * 2 + c)
        n_pass(dz).start()
    for dz in range(HI):
        n_wait(((hi - dz + HI) % HI) * 2 + other)
    for dz in range(HI):
        row = ((hi - dz + HI) % HI) * LO
        up_wait(row + lo2)
        up_wait(row + lo3)
        dn_wait(row + lo1)
        dn_wait(row + lo3)

    step = 256 if CH % 256 == 0 else LANES
    for i in range(CH // step):
        cols = slice(i * step, (i + 1) * step)
        raw = jnp.maximum(jnp.dot(n_buf[...], up_buf[:, cols], preferred_element_type=F32), 0.0)
        hid_buf[:, cols] = (raw * raw).astype(BF16)
    W = dn_ref.shape[1]

    @pl.loop(0, HI * LO)
    def _(j):
        cols = pl.ds(pl.multiple_of(j * W, LANES), W)
        part = jnp.dot(hid_buf[...], dn_buf[j], preferred_element_type=F32)
        ps_buf[:, cols] = part.astype(BF16)

    def p_out(dz, dc):
        i = ((hi + dz) % HI) * 2 + (c + dc) % 2
        return remote(
            ps_buf.at[pl.ds(i * H, H)],
            pr_buf.at[me],
            p_send.at[2 * dz + dc],
            p_recv.at[me],
            ((hi + dz) % HI) * LO + lo,
            (c + dc) % 2,
        )

    pairs = [(dz, dc) for dz in range(HI) for dc in range(2) if dz + dc > 0]
    for dz, dc in pairs:
        p_out(dz, dc).start()
    update = ps_buf[pl.ds(me * H, H), :].astype(F32)
    for dz, dc in pairs:
        i = ((hi - dz + HI) % HI) * 2 + (c + dc) % 2
        remote(pr_buf.at[i], pr_buf.at[i], p_send.at[0], p_recv.at[i], s, other).wait_recv()
        update = update + pr_buf[i].astype(F32)
    out_ref[...] = (res_buf[...].astype(F32) + update).astype(BF16)

    for hp in range(HI):

        @pl.when(hp > hi)
        def _():
            kv_up(hp).wait_send()

        @pl.when(hp <= hi)
        def _():
            for k in range(3):
                kv_flat(hp, k, kvb_ref).wait_send()

    for dz in range(HI):
        if dz > 0:
            for copy in w_far(dz):
                copy.wait_send()
            n_out(dz).wait_send()
        n_pass(dz).wait_send()
        for copy in w_flat(dz):
            copy.wait_send()
        for copy in w_diag(dz):
            copy.wait_send()
    for dz, dc in pairs:
        p_out(dz, dc).wait_send()


def fits(tokens, queries, key_values, stop_bias, up_proj, down_proj):
    sp = lax.axis_size("sp")
    rows, seqs, heads = stop_bias.shape
    hidden = up_proj.shape[1]
    return (
        lax.axis_size("tp") == 2
        and sp % LO == 0
        and seqs == 1
        and heads <= LANES
        and queries.shape[2] == heads * HEAD
        and key_values.shape[2] == heads * HEAD
        and 2 * HEAD == LANES
        and 2 * rows == LANES
        and hidden % (sp // LO * LANES) == 0
        and down_proj.shape[1] % LANES == 0
        and up_proj.shape[0] % 16 == 0
        and tokens.shape[2] % LANES == 0
    )


def body(tokens, queries, key_values, stop_bias, out_proj, norm_gain, up_proj, down_proj):
    if not fits(tokens, queries, key_values, stop_bias, up_proj, down_proj):
        return general_body(
            tokens, queries, key_values, stop_bias, out_proj, norm_gain, up_proj, down_proj
        )
    sp = lax.axis_size("sp")
    HI = sp // LO
    T, _, D = tokens.shape
    H = T // 2
    heads = stop_bias.shape[2]
    G = heads // 2
    R, hidden = up_proj.shape
    CH = hidden // HI
    W = down_proj.shape[1]
    kvb = jnp.concatenate(
        [
            key_values.reshape(T, key_values.shape[2]),
            jnp.pad(stop_bias.reshape(T, heads), ((0, 0), (0, LANES - heads))),
        ],
        axis=1,
    )
    KB = kvb.shape[1]
    vmem = pl.BlockSpec(memory_space=pltpu.VMEM)
    dma = pltpu.SemaphoreType.DMA
    out = pl.pallas_call(
        lambda *refs: layer_kernel(HI, G, *refs),
        out_shape=jax.ShapeDtypeStruct((H, D), BF16),
        in_specs=[vmem] * 7,
        out_specs=vmem,
        scratch_shapes=[
            pltpu.VMEM((sp * T, KB), BF16),
            pltpu.VMEM((sp * R, CH), BF16),
            pltpu.VMEM((sp, CH, W), BF16),
            pltpu.VMEM((G, LANES, LANES), BF16),
            pltpu.VMEM((LO * T, LO * T), BF16),
            pltpu.VMEM((G, 1, LANES), F32),
            pltpu.VMEM((G, LANES, LANES), F32),
            pltpu.VMEM((T, G * LANES), BF16),
            pltpu.VMEM((T, D), BF16),
            pltpu.VMEM((H, D), BF16),
            pltpu.VMEM((H, D), BF16),
            pltpu.VMEM((HI * T, D), BF16),
            pltpu.VMEM((HI * T, CH), BF16),
            pltpu.VMEM((HI * T, D), BF16),
            pltpu.VMEM((HI * 2, H, D), BF16),
            dma((HI,)),
            dma((HI * 3,)),
            dma((sp,)),
            dma((HI * 2,)),
            dma((HI * 6,)),
            dma((sp,)),
            dma((sp,)),
            dma,
            dma,
            dma((HI,)),
            dma((HI,)),
            dma((HI * 2,)),
            dma((HI * 2,)),
            dma((HI * 2,)),
        ],
        compiler_params=pltpu.CompilerParams(
            collective_id=0, has_side_effects=True, vmem_limit_bytes=56 * 1024 * 1024
        ),
        name="layer",
    )(
        tokens.reshape(T, D),
        queries.reshape(T, queries.shape[2]),
        kvb,
        out_proj,
        norm_gain.reshape(1, D),
        up_proj,
        down_proj,
    )
    return out.reshape(H, 1, D)


def solution(mesh):
    return jax.shard_map(
        body,
        mesh=mesh,
        in_specs=(
            P("sp", None, None),
            P("sp", None, "tp"),
            P("sp", None, "tp"),
            P("sp", None, "tp"),
            P("tp", None),
            P(),
            P("sp", "tp"),
            P("tp", "sp"),
        ),
        out_specs=P(("sp", "tp"), None, None),
        check_vma=False,
    )
```

profile of v0, /device:TPU:9, one launch (start us, length us, event | category | flops | bytes accessed | tf_op | source)
XLA Modules:
  0.0 96.0 jit_solution(15551147399975799234)
XLA Ops:
  0.0 0.8 copy.9
  0.8 1.5 %fusion.1.refs_2_ = bf16[64,640]{1,0:T(8,128)(2,1)} fusion(bf16[64,8]{1,0:T(8,128)(2,1)S(1)} %bitcast.9, bf16[64,512]{1,0:T(8,128)(2,1)} %bitcast.10), kind=kLoop, calls=%fused_computation.2 | loop fusion | flops 245760 | bytes 148480 | tf_op jit(solution)/shard_map/concatenate | solution.py:584
  2.3 92.1 %layer.1 = bf16[32,2048]{1,0:T(8,128)(2,1)} custom-call(bf16[64,2048]{1,0:T(8,128)(2,1)} %bitcast.7, bf16[64,512]{1,0:T(8,128)(2,1)} %bitcast.8, bf16[64,640]{1,0:T(8,128)(2,1)} %fusion.1.refs_2_, bf16[512,2048]{1,0:T(8,128)(2,1)} %refs_3_.1, f32[1,2048]{1,0:T(1,128)} %bitcast.11, bf16[128,2048]{1,0:T(8,128)(2,1)} %refs_5_.1, bf16[2048,128]{1,0:T(8,128)(2,1)} %refs_6_.1), custom_call_target="tpu_custom_call" | custom-call | tf_op jit(solution)/shard_map/layer/pallas_call | solution.py:594
  94.4 1.6 %copy.11 = bf16[32,1,2048]{2,0,1:T(8,128)(2,1)} copy(bf16[32,1,2048]{2,0,1:T(8,128)(2,1)} %bitcast.6) | data formatting | bytes 262144
where the time goes:
time: 96.2 us; the launch traced here: 96 us
  Pallas kernels  92.1 us (96%)
  local copies, waits for them, and re-layouts  2.34 us (2%)
  other arithmetic  1.48 us (2%)
    pallas_call x1, Pallas kernels, body(): pl.pallas_call(lambda *refs: layer_kernel(HI, G, *refs), out_shape=jax.Sh...  92.1 us
    unnamed x2, local copies, waits for them, and re-layouts  2.34 us

commit v1 on v0

--- a/solution.py
+++ b/solution.py
@@ -215,19 +215,27 @@
     n_buf,
     hid_buf,
     ps_buf,
+    x_in,
+    xs_buf,
     pr_buf,
     kv_sz,
     kv_sp,
     kv_recv,
+    kv_half,
     wz_send,
-    wp_send,
+    up_sp,
     up_recv,
+    up_half,
+    dn_sp,
     dn_recv,
+    dn_half,
     pj_send,
     pj_recv,
     n_send,
     nf_send,
     n_recv,
+    x_send,
+    x_recv,
     p_send,
     p_recv,
 ):
@@ -244,103 +252,86 @@
     D = tok_ref.shape[1]
     R = up_ref.shape[0]
     CH = up_buf.shape[1]
+    W = dn_ref.shape[1]
     KW = G * LANES
     PL = LO * T
+    own_cols = pl.ds(pl.multiple_of(hi * CH, LANES), CH)
 
     barrier = pltpu.get_barrier_semaphore()
-    for p in (lo1, lo2, lo3):
+    for p in (lo1, lo2):
         pl.semaphore_signal(barrier, inc=1, device_id={"sp": hi * LO + p, "tp": c}, device_id_type=MESH)
     pl.semaphore_signal(barrier, inc=1, device_id={"sp": s, "tp": other}, device_id_type=MESH)
     for dz in range(1, HI):
         far = ((hi + dz) % HI) * LO + lo
-        for core in range(2):
-            pl.semaphore_signal(barrier, inc=1, device_id={"sp": far, "tp": core}, device_id_type=MESH)
-    pl.semaphore_wait(barrier, 4 + 2 * (HI - 1))
+        pl.semaphore_signal(barrier, inc=1, device_id={"sp": far, "tp": c}, device_id_type=MESH)
+    pl.semaphore_wait(barrier, 3 + (HI - 1))
+
+    class Piece:
+        def __init__(self, view, rows, send, recv, half):
+            self.view, self.rows, self.send, self.recv, self.half = view, rows, send, recv, half
+
+        def full(self, j):
+            return self.view(j, 0, self.rows)
+
+        def part(self, j, h):
+            return self.view(j, h * (self.rows // 2), self.rows // 2)
+
+        def direct(self, z, src=None):
+            j = z * LO + lo
+            src = self.full(j) if src is None else src
+            return [
+                remote(src, self.full(j), self.send.at[z * 4 + k], self.recv.at[j], hi * LO + p, c)
+                for k, p in enumerate((lo1, lo2))
+            ]
+
+        def diag(self, z):
+            a, b = z * LO + lo1, z * LO + lo2
+            first, last = self.part(a, 0), self.part(b, 1)
+            return [
+                remote(first, first, self.send.at[z * 4 + 2], self.recv.at[a], hi * LO + lo2, c),
+                remote(last, last, self.send.at[z * 4 + 3], self.half.at[z], hi * LO + lo1, c),
+            ]
+
+        def arrived(self, ref, sem):
+            remote(ref, ref, self.send.at[0], sem, s, other).wait_recv()
+
+        def wait_own(self, z):
+            j = z * LO + lo
+            self.arrived(self.full(j), self.recv.at[j])
+
+        def wait_direct(self, z):
+            for p in (lo1, lo2):
+                j = z * LO + p
+                self.arrived(self.full(j), self.recv.at[j])
+
+        def wait_diag(self, z):
+            j = z * LO + lo3
+            self.arrived(self.part(j, 0), self.recv.at[j])
+            self.arrived(self.part(j, 1), self.half.at[z])
+
+    kv = Piece(lambda j, r, n: kv_buf.at[pl.ds(j * T + r, n)], T, kv_sp, kv_recv, kv_half)
+    up = Piece(lambda j, r, n: up_buf.at[pl.ds(j * R + r, n)], R, up_sp, up_recv, up_half)
+    dn = Piece(lambda j, r, n: dn_buf.at[j, pl.ds(r, n)], CH, dn_sp, dn_recv, dn_half)
+    up_own = up_ref.at[:, own_cols]
+    dn_own = dn_ref.at[pl.ds(hi * CH, CH)]
+
+    def start(copies):
+        for copy in copies:
+            copy.start()
+
+    def below(dz):
+        return (hi - dz + HI) % HI
 
     def kv_up(hp):
-        return remote(
-            kvb_ref, kv_buf.at[pl.ds(s * T, T)], kv_sz.at[hp], kv_recv.at[s], hp * LO + lo, c
-        )
-
-    def kv_flat(hp, k, src):
-        j = hp * LO + lo
-        peer = (lo1, lo2, lo3)[k]
-        return remote(
-            src, kv_buf.at[pl.ds(j * T, T)], kv_sp.at[hp * 3 + k], kv_recv.at[j], hi * LO + peer, c
-        )
-
-    def kv_wait(j):
-        block = kv_buf.at[pl.ds(j * T, T)]
-        remote(block, block, kv_sz.at[0], kv_recv.at[j], s, other).wait_recv()
-
-    def w_far(dz):
-        hp = (hi + dz) % HI
-        far = hp * LO + lo
-        return (
-            remote(
-                up_ref.at[:, pl.ds(pl.multiple_of(hp * CH, LANES), CH)],
-                up_buf.at[pl.ds(s * R, R)],
-                wz_send.at[2 * dz],
-                up_recv.at[s],
-                far,
-                c,
-            ),
-            remote(
-                dn_ref.at[pl.ds(hp * CH, CH)],
-                dn_buf.at[s],
-                wz_send.at[2 * dz + 1],
-                dn_recv.at[s],
-                far,
-                c,
-            ),
-        )
-
-    def up_at(j):
-        return up_buf.at[pl.ds(j * R, R)]
-
-    def up_wait(j):
-        remote(up_at(j), up_at(j), wz_send.at[0], up_recv.at[j], s, other).wait_recv()
-
-    def dn_wait(j):
-        remote(dn_buf.at[j], dn_buf.at[j], wz_send.at[0], dn_recv.at[j], s, other).wait_recv()
-
-    def w_flat(dz):
-        j = ((hi - dz + HI) % HI) * LO + lo
-        if dz == 0:
-            up_src = up_ref.at[:, pl.ds(pl.multiple_of(hi * CH, LANES), CH)]
-            dn_src = dn_ref.at[pl.ds(hi * CH, CH)]
-        else:
-            up_src = up_at(j)
-            dn_src = dn_buf.at[j]
-        copies = []
-        for k, peer in enumerate((lo1, lo2)):
-            far = hi * LO + peer
-            copies.append(remote(up_src, up_at(j), wp_send.at[6 * dz + 2 * k], up_recv.at[j], far, c))
-            copies.append(
-                remote(dn_src, dn_buf.at[j], wp_send.at[6 * dz + 2 * k + 1], dn_recv.at[j], far, c)
-            )
-        return copies
-
-    def w_diag(dz):
-        row = ((hi - dz + HI) % HI) * LO
-        return (
-            remote(
-                up_at(row + lo1),
-                up_at(row + lo1),
-                wp_send.at[6 * dz + 4],
-                up_recv.at[row + lo1],
-                hi * LO + lo2,
-                c,
-            ),
-            remote(
-                dn_buf.at[row + lo2],
-                dn_buf.at[row + lo2],
-                wp_send.at[6 * dz + 5],
-                dn_recv.at[row + lo2],
-                hi * LO + lo1,
-                c,
-            ),
-        )
+        return remote(kvb_ref, kv.full(s), kv_sz.at[hp], kv_recv.at[s], hp * LO + lo, c)
+
+    def up_far(hp):
+        cols = pl.ds(hp * CH, CH)
+        return remote(up_ref.at[:, cols], up.full(s), wz_send.at[2 * hp], up_recv.at[s], hp * LO + lo, c)
+
+    def dn_far(hp):
+        rows = pl.ds(hp * CH, CH)
+        return remote(dn_ref.at[rows], dn.full(s), wz_send.at[2 * hp + 1], dn_recv.at[s], hp * LO + lo, c)
 
     for hp in range(HI):
 
@@ -348,23 +339,16 @@
         def _():
             kv_up(hp).start()
 
-    for hp in range(HI):
-
-        @pl.when(hp == hi)
-        def _():
-            for k in range(3):
-                kv_flat(hp, k, kvb_ref).start()
-
-    for dz in range(1, HI):
-        for copy in w_far(dz):
-            copy.start()
-
+    start(kv.direct(hi, kvb_ref))
+    for far in (up_far, dn_far):
+        for hp in range(HI - 2, -1, -1):
+
+            @pl.when(hp < hi)
+            def _():
+                far(hp).start()
+
+    start(up.direct(hi, up_own))
     kv_buf[pl.ds(s * T, T), :] = kvb_ref[...]
-    up_buf[pl.ds(s * R, R), :] = up_ref[:, pl.ds(pl.multiple_of(hi * CH, LANES), CH)]
-    dn_buf[s] = dn_ref[pl.ds(hi * CH, CH), :]
-    row_id = lax.broadcasted_iota(jnp.int32, (PL, PL), 0)
-    col_id = lax.broadcasted_iota(jnp.int32, (PL, PL), 1)
-    tri_buf[...] = jnp.where(col_id > row_id, 1.0, 0.0).astype(BF16)
     lane = lax.broadcasted_iota(jnp.int32, (T, LANES), 1)
     low = lane < HEAD
     for g in range(G):
@@ -372,19 +356,11 @@
         first = jnp.where(low, qg, 0.0)
         second = jnp.where(low, pltpu.roll(qg, HEAD, 1), 0.0)
         q_buf[g] = jnp.concatenate([first, second], axis=0).astype(BF16)
+    row_id = lax.broadcasted_iota(jnp.int32, (PL, PL), 0)
+    col_id = lax.broadcasted_iota(jnp.int32, (PL, PL), 1)
+    tri_buf[...] = jnp.where(col_id > row_id, 1.0, 0.0).astype(BF16)
     carry[...] = jnp.zeros_like(carry)
     acc[...] = jnp.zeros_like(acc)
-
-    for hp in range(HI - 1):
-
-        @pl.when(hp < hi)
-        def _():
-            kv_wait(hp * LO + lo)
-            for k in range(3):
-                kv_flat(hp, k, kv_buf.at[pl.ds((hp * LO + lo) * T, T)]).start()
-
-    for copy in w_flat(0):
-        copy.start()
 
     sel_row = lax.broadcasted_iota(jnp.int32, (LANES, LANES), 0) // HEAD
     sel_lane = lax.broadcasted_iota(jnp.int32, (LANES, LANES), 1)
@@ -392,15 +368,13 @@
     query_pos = s * T + lax.broadcasted_iota(jnp.int32, (PL, LANES), 1) % T
 
     def attend(plane):
-        for p in (lo1, lo2, lo3):
-            kv_wait(plane * LO + p)
         rows = pl.ds(plane * PL, PL)
         bias = kv_buf[rows, KW : KW + LANES]
         strict = plane * PL + key_row < query_pos
         for g in range(G):
-            kv = kv_buf[rows, g * LANES : (g + 1) * LANES]
+            pairs = kv_buf[rows, g * LANES : (g + 1) * LANES]
             pick = jnp.where(sel_lane == 2 * g + sel_row, 1.0, 0.0).astype(BF16)
-            scores = dot_nt(kv, q_buf[g]) + dot_nt(bias, pick)
+            scores = dot_nt(pairs, q_buf[g]) + dot_nt(bias, pick)
             soft = jnp.maximum(scores, 0.0) + jnp.log(1.0 + jnp.exp(-jnp.abs(scores)))
             log_pass = jnp.where(strict, -soft, 0.0)
             top = log_pass.astype(BF16)
@@ -410,21 +384,68 @@
             )
             held = carry[g]
             weights = jnp.where(strict, jnp.exp(scores - soft + after + held), 0.0).astype(BF16)
-            acc[g] += dot_tn(weights, kv)
+            acc[g] += dot_tn(weights, pairs)
             carry[g] = held + after[0:1] + log_pass[0:1]
 
-    for k in range(HI):
-
+    def column(k):
         @pl.when(k <= hi)
         def _():
+            kv.wait_own(hi - k)
+            start(kv.direct(hi - k))
+
+    def relay(k):
+        @pl.when(k <= hi)
+        def _():
+            kv.wait_direct(hi - k)
+            start(kv.diag(hi - k))
+
+    def look(k):
+        @pl.when(k <= hi)
+        def _():
+            kv.wait_diag(hi - k)
             attend(hi - k)
 
-        if k + 1 < HI:
-            j = ((hi - k - 1 + HI) % HI) * LO + lo
-            up_wait(j)
-            dn_wait(j)
-            for copy in w_flat(k + 1):
-                copy.start()
+    def up_column(dz):
+        up.wait_own(below(dz))
+        start(up.direct(below(dz)))
+
+    def up_relay(dz):
+        up.wait_direct(below(dz))
+        start(up.diag(below(dz)))
+
+    def dn_column(dz):
+        dn.wait_own(below(dz))
+        start(dn.direct(below(dz)))
+
+    def dn_relay(dz):
+        dn.wait_direct(below(dz))
+        start(dn.diag(below(dz)))
+
+    for k in range(1, HI):
+        column(k)
+        relay(k - 1)
+        if k == 1:
+            for far in (up_far, dn_far):
+                for hp in range(1, HI):
+
+                    @pl.when(hp > hi)
+                    def _():
+                        far(hp).start()
+
+            up_buf[pl.ds(s * R, R), :] = up_ref[:, own_cols]
+            dn_buf[s] = dn_ref[pl.ds(hi * CH, CH), :]
+        if k >= 2:
+            look(k - 2)
+    relay(HI - 1)
+    up_column(1)
+    up_relay(0)
+    if HI >= 2:
+        look(HI - 2)
+    for dz in range(2, HI):
+        up_column(dz)
+    start(dn.direct(hi, dn_own))
+    look(HI - 1)
+    up_relay(1)
 
     for g in range(G):
         a0 = pltpu.roll(acc[g, 0:T, :], HEAD, 1)
@@ -432,15 +453,14 @@
         att_buf[:, g * LANES : (g + 1) * LANES] = jnp.where(low, a0, a1).astype(BF16)
     att = att_buf[...]
     wide = 512 if D % 512 == 0 else LANES
-
-    @pl.loop(0, D // wide)
-    def _(i):
-        cols = pl.ds(pl.multiple_of(i * wide, wide), wide)
-        part = jnp.dot(att, wo_ref[:, cols], preferred_element_type=F32)
-        pj_buf[:, cols] = part.astype(BF16)
+    for i in range(D // wide):
+        cols = slice(i * wide, (i + 1) * wide)
+        pj_buf[:, cols] = jnp.dot(att, wo_ref[:, cols], preferred_element_type=F32).astype(BF16)
 
     pj_copy = remote(pj_buf.at[pl.ds(other * H, H)], pj_in, pj_send, pj_recv, s, other)
     pj_copy.start()
+    for dz in range(2, HI):
+        up_relay(dz)
     pj_copy.wait()
     mine = pl.ds(c * H, H)
     total = pj_buf[mine, :].astype(F32) + pj_in[...].astype(F32)
@@ -448,79 +468,97 @@
     res_buf[...] = residual
     values = residual.astype(F32)
     factor = lax.rsqrt(jnp.mean(values * values, axis=-1, keepdims=True) + EPSILON)
-    me = hi * 2 + c
-
-    def n_at(i):
-        return n_buf.at[pl.ds(i * H, H)]
-
-    n_buf[pl.ds(me * H, H), :] = (values * factor * gain_ref[...]).astype(BF16)
+
+    def n_at(z, core):
+        return n_buf.at[pl.ds((core * HI + z) * H, H)]
+
+    n_buf[pl.ds((c * HI + hi) * H, H), :] = (values * factor * gain_ref[...]).astype(BF16)
 
     def n_out(dz):
         hp = (hi + dz) % HI
-        return remote(n_at(me), n_at(me), n_send.at[dz], n_recv.at[me], hp * LO + lo, c)
+        return remote(n_at(hi, c), n_at(hi, c), n_send.at[dz], n_recv.at[c * HI + hi], hp * LO + lo, c)
 
     def n_pass(dz):
-        i = ((hi - dz + HI) % HI) * 2 + c
-        return remote(n_at(i), n_at(i), nf_send.at[dz], n_recv.at[i], s, other)
-
-    def n_wait(i):
-        remote(n_at(i), n_at(i), nf_send.at[0], n_recv.at[i], s, other).wait_recv()
+        z = below(dz)
+        return remote(n_at(z, c), n_at(z, c), nf_send.at[dz], n_recv.at[c * HI + z], s, other)
+
+    def n_wait(z, core):
+        ref = n_at(z, core)
+        remote(ref, ref, nf_send.at[0], n_recv.at[core * HI + z], s, other).wait_recv()
 
     for dz in range(1, HI):
         n_out(dz).start()
     n_pass(0).start()
-
-    for dz in range(HI):
-        row = ((hi - dz + HI) % HI) * LO
-        up_wait(row + lo1)
-        dn_wait(row + lo2)
-        for copy in w_diag(dz):
-            copy.start()
     for dz in range(1, HI):
-        n_wait(((hi - dz + HI) % HI) * 2 + c)
+        dn_column(dz)
+    dn_relay(0)
+    for dz in range(1, HI):
+        n_wait(below(dz), c)
         n_pass(dz).start()
     for dz in range(HI):
-        n_wait(((hi - dz + HI) % HI) * 2 + other)
+        up.wait_diag(below(dz))
     for dz in range(HI):
-        row = ((hi - dz + HI) % HI) * LO
-        up_wait(row + lo2)
-        up_wait(row + lo3)
-        dn_wait(row + lo1)
-        dn_wait(row + lo3)
+        n_wait(below(dz), other)
 
     step = 256 if CH % 256 == 0 else LANES
     for i in range(CH // step):
         cols = slice(i * step, (i + 1) * step)
         raw = jnp.maximum(jnp.dot(n_buf[...], up_buf[:, cols], preferred_element_type=F32), 0.0)
         hid_buf[:, cols] = (raw * raw).astype(BF16)
-    W = dn_ref.shape[1]
-
-    @pl.loop(0, HI * LO)
-    def _(j):
-        cols = pl.ds(pl.multiple_of(j * W, LANES), W)
-        part = jnp.dot(hid_buf[...], dn_buf[j], preferred_element_type=F32)
-        ps_buf[:, cols] = part.astype(BF16)
-
-    def p_out(dz, dc):
-        i = ((hi + dz) % HI) * 2 + (c + dc) % 2
+
+    half = HI * H
+
+    def x_out(dz):
+        z = below(dz)
+        rows = pl.ds(other * half, half)
+        return remote(ps_buf.at[z, rows], x_in.at[z], x_send.at[dz], x_recv.at[z], s, other)
+
+    def p_out(dz, far):
+        z = below(dz)
+        hp = (hi + far) % HI
         return remote(
-            ps_buf.at[pl.ds(i * H, H)],
-            pr_buf.at[me],
-            p_send.at[2 * dz + dc],
-            p_recv.at[me],
-            ((hi + dz) % HI) * LO + lo,
-            (c + dc) % 2,
+            xs_buf.at[z, pl.ds(hp * H, H)],
+            pr_buf.at[hi, z],
+            p_send.at[dz * HI + far],
+            p_recv.at[hi * HI + z],
+            hp * LO + lo,
+            c,
         )
 
-    pairs = [(dz, dc) for dz in range(HI) for dc in range(2) if dz + dc > 0]
-    for dz, dc in pairs:
-        p_out(dz, dc).start()
-    update = ps_buf[pl.ds(me * H, H), :].astype(F32)
-    for dz, dc in pairs:
-        i = ((hi - dz + HI) % HI) * 2 + (c + dc) % 2
-        remote(pr_buf.at[i], pr_buf.at[i], p_send.at[0], p_recv.at[i], s, other).wait_recv()
-        update = update + pr_buf[i].astype(F32)
-    out_ref[...] = (res_buf[...].astype(F32) + update).astype(BF16)
+    def p_wait(src, z):
+        ref = pr_buf.at[src, z]
+        remote(ref, ref, p_send.at[0], p_recv.at[src * HI + z], s, other).wait_recv()
+
+    def spread(dz):
+        z = below(dz)
+        x_in_ref = x_in.at[z]
+        remote(x_in_ref, x_in_ref, x_send.at[0], x_recv.at[z], s, other).wait_recv()
+        mixed = ps_buf[z, pl.ds(c * half, half), :].astype(F32) + x_in[z].astype(F32)
+        xs_buf[z] = mixed.astype(BF16)
+        for far in range(1, HI):
+            p_out(dz, far).start()
+
+    for dz in range(HI):
+        if dz + 1 < HI:
+            dn_relay(dz + 1)
+        z = below(dz)
+        dn.wait_diag(z)
+        for q in range(LO):
+            part = jnp.dot(hid_buf[...], dn_buf[z * LO + q], preferred_element_type=F32)
+            ps_buf[z, :, q * W : (q + 1) * W] = part.astype(BF16)
+        x_out(dz).start()
+        if dz > 0:
+            spread(dz - 1)
+    spread(HI - 1)
+    CW = LO * W
+    for dz in range(HI):
+        z = below(dz)
+        cols = pl.ds(pl.multiple_of(z * CW, LANES), CW)
+        update = xs_buf[z, pl.ds(hi * H, H), :].astype(F32)
+        for far in range(1, HI):
+            p_wait(below(far), z)
+            update = update + pr_buf[below(far), z].astype(F32)
+        out_ref[:, cols] = (res_buf[:, cols].astype(F32) + update).astype(BF16)
 
     for hp in range(HI):
 
@@ -530,21 +568,24 @@
 
         @pl.when(hp <= hi)
         def _():
-            for k in range(3):
-                kv_flat(hp, k, kvb_ref).wait_send()
+            for copy in kv.direct(hp) + kv.diag(hp):
+                copy.wait_send()
+
+        @pl.when(hp != hi)
+        def _():
+            up_far(hp).wait_send()
+            dn_far(hp).wait_send()
+
+        for copy in up.direct(hp) + up.diag(hp) + dn.direct(hp) + dn.diag(hp):
+            copy.wait_send()
 
     for dz in range(HI):
+        n_pass(dz).wait_send()
+        x_out(dz).wait_send()
         if dz > 0:
-            for copy in w_far(dz):
-                copy.wait_send()
             n_out(dz).wait_send()
-        n_pass(dz).wait_send()
-        for copy in w_flat(dz):
-            copy.wait_send()
-        for copy in w_diag(dz):
-            copy.wait_send()
-    for dz, dc in pairs:
-        p_out(dz, dc).wait_send()
+        for far in range(1, HI):
+            p_out(dz, far).wait_send()
 
 
 def fits(tokens, queries, key_values, stop_bias, up_proj, down_proj):
@@ -554,6 +595,7 @@
     return (
         lax.axis_size("tp") == 2
         and sp % LO == 0
+        and sp > LO
         and seqs == 1
         and heads <= LANES
         and queries.shape[2] == heads * HEAD
@@ -610,22 +652,30 @@
             pltpu.VMEM((H, D), BF16),
             pltpu.VMEM((HI * T, D), BF16),
             pltpu.VMEM((HI * T, CH), BF16),
-            pltpu.VMEM((HI * T, D), BF16),
-            pltpu.VMEM((HI * 2, H, D), BF16),
+            pltpu.VMEM((HI, HI * T, LO * W), BF16),
+            pltpu.VMEM((HI, HI * H, LO * W), BF16),
+            pltpu.VMEM((HI, HI * H, LO * W), BF16),
+            pltpu.VMEM((HI, HI, H, LO * W), BF16),
             dma((HI,)),
-            dma((HI * 3,)),
+            dma((HI * 4,)),
             dma((sp,)),
+            dma((HI,)),
             dma((HI * 2,)),
-            dma((HI * 6,)),
+            dma((HI * 4,)),
             dma((sp,)),
+            dma((HI,)),
+            dma((HI * 4,)),
             dma((sp,)),
+            dma((HI,)),
             dma,
             dma,
             dma((HI,)),
             dma((HI,)),
             dma((HI * 2,)),
-            dma((HI * 2,)),
-            dma((HI * 2,)),
+            dma((HI,)),
+            dma((HI,)),
+            dma((HI * HI,)),
+            dma((HI * HI,)),
         ],
         compiler_params=pltpu.CompilerParams(
             collective_id=0, has_side_effects=True, vmem_limit_bytes=56 * 1024 * 1024

time: 96.2 us -> 76.2 us (0.79)
  the two profiles are of different devices: /device:TPU:9 before, /device:TPU:0 now
where the time goes in v1:
time: 76.2 us; the launch traced here: 76 us
  Pallas kernels  72.2 us (95%)
  local copies, waits for them, and re-layouts  2.34 us (3%)
  other arithmetic  1.48 us (2%)
    pallas_call x1, Pallas kernels, body(): pl.pallas_call(lambda *refs: layer_kernel(HI, G, *refs), out_shape=jax.Sh...  72.2 us
    unnamed x2, local copies, waits for them, and re-layouts  2.34 us

profile of v1, /device:TPU:0, one launch (start us, length us, event | category | flops | bytes accessed | tf_op | source)
XLA Modules:
  0.0 76.0 jit_solution(9556622398155899115)
XLA Ops:
  0.0 0.8 %copy.9 = bf16[64,1,8]{2,0,1:T(8,128)(2,1)S(1)} copy(bf16[64,1,8]{0,2,1:T(8,128)(2,1)} %param.11) | data formatting | bytes 2048 | tf_op args[3]
  0.8 1.5 %fusion.1.refs_2_ = bf16[64,640]{1,0:T(8,128)(2,1)} fusion(bf16[64,8]{1,0:T(8,128)(2,1)S(1)} %bitcast.9, bf16[64,512]{1,0:T(8,128)(2,1)} %bitcast.10), kind=kLoop, calls=%fused_computation.2 | loop fusion | flops 245760 | bytes 148480 | tf_op jit(solution)/shard_map/concatenate | solution.py:626
  2.3 72.2 %layer.1 = bf16[32,2048]{1,0:T(8,128)(2,1)} custom-call(bf16[64,2048]{1,0:T(8,128)(2,1)} %bitcast.7, bf16[64,512]{1,0:T(8,128)(2,1)} %bitcast.8, bf16[64,640]{1,0:T(8,128)(2,1)} %fusion.1.refs_2_, bf16[512,2048]{1,0:T(8,128)(2,1)} %refs_3_.1, f32[1,2048]{1,0:T(1,128)} %bitcast.11, bf16[128,2048]{1,0:T(8,128)(2,1)} %refs_5_.1, bf16[2048,128]{1,0:T(8,128)(2,1)} %refs_6_.1), custom_call_target="tpu_custom_call" | custom-call | tf_op jit(solution)/shard_map/layer/pallas_call | solution.py:636
  74.5 1.6 %copy.11 = bf16[32,1,2048]{2,0,1:T(8,128)(2,1)} copy(bf16[32,1,2048]{2,0,1:T(8,128)(2,1)} %bitcast.6) | data formatting | bytes 262144

commit v2 on v1

--- a/solution.py
+++ b/solution.py
@@ -195,12 +195,16 @@
     G,
     tok_ref,
     q_ref,
-    kvb_ref,
-    wo_ref,
+    kvp_ref,
+    bias_ref,
+    wo_hbm,
     gain_ref,
     up_ref,
     dn_ref,
     out_ref,
+    kvb_ref,
+    wo_ref,
+    load_sem,
     kv_buf,
     up_buf,
     dn_buf,
@@ -264,6 +268,16 @@
     for dz in range(1, HI):
         far = ((hi + dz) % HI) * LO + lo
         pl.semaphore_signal(barrier, inc=1, device_id={"sp": far, "tp": c}, device_id_type=MESH)
+    loads = [
+        pltpu.make_async_copy(wo_hbm, wo_ref, load_sem.at[0]),
+        pltpu.make_async_copy(up_ref.at[:, own_cols], up_buf.at[pl.ds(s * R, R)], load_sem.at[1]),
+        pltpu.make_async_copy(dn_ref.at[pl.ds(hi * CH, CH)], dn_buf.at[s], load_sem.at[2]),
+    ]
+    for load in loads:
+        load.start()
+    kvb_ref[:, :KW] = kvp_ref[...]
+    kvb_ref[:, KW:] = jnp.zeros((T, LANES), BF16)
+    kvb_ref[:, KW : KW + 2 * G] = bias_ref[...]
     pl.semaphore_wait(barrier, 3 + (HI - 1))
 
     class Piece:
@@ -432,8 +446,6 @@
                     def _():
                         far(hp).start()
 
-            up_buf[pl.ds(s * R, R), :] = up_ref[:, own_cols]
-            dn_buf[s] = dn_ref[pl.ds(hi * CH, CH), :]
         if k >= 2:
             look(k - 2)
     relay(HI - 1)
@@ -447,6 +459,8 @@
     look(HI - 1)
     up_relay(1)
 
+    for load in loads:
+        load.wait()
     for g in range(G):
         a0 = pltpu.roll(acc[g, 0:T, :], HEAD, 1)
         a1 = acc[g, T : 2 * T, :]
@@ -543,9 +557,10 @@
             dn_relay(dz + 1)
         z = below(dz)
         dn.wait_diag(z)
-        for q in range(LO):
-            part = jnp.dot(hid_buf[...], dn_buf[z * LO + q], preferred_element_type=F32)
-            ps_buf[z, :, q * W : (q + 1) * W] = part.astype(BF16)
+        for q in range(0, LO, 2):
+            pair = jnp.concatenate([dn_buf[z * LO + q], dn_buf[z * LO + q + 1]], axis=1)
+            part = jnp.dot(hid_buf[...], pair, preferred_element_type=F32)
+            ps_buf[z, :, q * W : (q + 2) * W] = part.astype(BF16)
         x_out(dz).start()
         if dz > 0:
             spread(dz - 1)
@@ -623,22 +638,19 @@
     R, hidden = up_proj.shape
     CH = hidden // HI
     W = down_proj.shape[1]
-    kvb = jnp.concatenate(
-        [
-            key_values.reshape(T, key_values.shape[2]),
-            jnp.pad(stop_bias.reshape(T, heads), ((0, 0), (0, LANES - heads))),
-        ],
-        axis=1,
-    )
-    KB = kvb.shape[1]
+    KB = G * LANES + LANES
     vmem = pl.BlockSpec(memory_space=pltpu.VMEM)
+    hbm = pl.BlockSpec(memory_space=pl.ANY)
     dma = pltpu.SemaphoreType.DMA
     out = pl.pallas_call(
         lambda *refs: layer_kernel(HI, G, *refs),
         out_shape=jax.ShapeDtypeStruct((H, D), BF16),
-        in_specs=[vmem] * 7,
+        in_specs=[vmem, vmem, vmem, vmem, hbm, vmem, hbm, hbm],
         out_specs=vmem,
         scratch_shapes=[
+            pltpu.VMEM((T, KB), BF16),
+            pltpu.VMEM(out_proj.shape, BF16),
+            dma((3,)),
             pltpu.VMEM((sp * T, KB), BF16),
             pltpu.VMEM((sp * R, CH), BF16),
             pltpu.VMEM((sp, CH, W), BF16),
@@ -684,7 +696,8 @@
     )(
         tokens.reshape(T, D),
         queries.reshape(T, queries.shape[2]),
-        kvb,
+        key_values.reshape(T, key_values.shape[2]),
+        stop_bias.reshape(T, heads),
         out_proj,
         norm_gain.reshape(1, D),
         up_proj,

time: 76.2 us -> 74.3 us (0.975)
  other arithmetic: 1.48 us -> 0 us
  Pallas kernels: 72.2 us -> 71.1 us
    concatenate x1 -> x0, other arithmetic: 1.48 us -> none  [body(): jnp.concatenate([key_values.reshape(T, key_values.shape[2]), jnp.pad(stop...]
    pallas_call x1, Pallas kernels: 72.2 us -> 71.1 us  [body(): pl.pallas_call(lambda *refs: layer_kernel(HI, G, *refs), out_shape=jax.Sh...]
where the time goes in v2:
time: 74.3 us; the launch traced here: 74.1 us
  Pallas kernels  71.1 us (96%)
  local copies, waits for them, and re-layouts  2.94 us (4%)
    pallas_call x1, Pallas kernels, body(): pl.pallas_call(lambda *refs: layer_kernel(HI, G, *refs), out_shape=jax.Sh...  71.1 us
    unnamed x2, local copies, waits for them, and re-layouts  2.94 us

profile of v2, /device:TPU:0, one launch (start us, length us, event | category | flops | bytes accessed | tf_op | source)
XLA Modules:
  0.0 74.1 jit_solution(169558143279739895)
XLA Ops:
  0.0 1.4 %copy.9 = bf16[64,1,8]{2,0,1:T(8,128)(2,1)} copy(bf16[64,1,8]{0,2,1:T(8,128)(2,1)} %param.11) | data formatting | bytes 2048 | tf_op args[3]
  1.4 71.1 %layer.1 = bf16[32,2048]{1,0:T(8,128)(2,1)} custom-call(bf16[64,2048]{1,0:T(8,128)(2,1)} %bitcast.7, bf16[64,512]{1,0:T(8,128)(2,1)} %bitcast.8, bf16[64,512]{1,0:T(8,128)(2,1)} %bitcast.9, bf16[64,8]{1,0:T(8,128)(2,1)} %bitcast.10, bf16[512,2048]{1,0:T(8,128)(2,1)} %refs_4_.1, f32[1,2048]{1,0:T(1,128)} %bitcast.11, bf16[128,2048]{1,0:T(8,128)(2,1)} %refs_6_.1, ...), custom_call_target="tpu_custom_call" | custom-call | tf_op jit(solution)/shard_map/layer/pallas_call | solution.py:645
  72.5 1.6 %copy.11 = bf16[32,1,2048]{2,0,1:T(8,128)(2,1)} copy(bf16[32,1,2048]{2,0,1:T(8,128)(2,1)} %bitcast.6) | data formatting | bytes 262144
